TPU v7x, 32 devices: a whole 2x2x4 slice. The times are simulated.
32 devices in a mesh: sp: 16 (over z, y, core), tp: 2 (over x).
Axes of the slice: x: 2, y: 2, z: 4, core: 2. Of those that a mesh axis runs over, the one named last changes fastest.
Arguments:
- incoming_activity: bfloat16 [8192, 2048], P(('sp', 'tp')), may hold values from -6 to 6
- entry_standardize_factor: bfloat16 [2048], replicated, may hold values from 0.099609375 to 1.8984375
- recursive_entry_matrix: bfloat16 [2048, 2048], P(None, 'tp'), may hold values from -0.125 to 0.125
- final_switch_matrix: bfloat16 [2048, 2048], P(None, 'tp'), may hold values from -0.125 to 0.125
- averaging_entry_matrix: bfloat16 [2048, 1024], P(None, 'tp'), may hold values from -0.125 to 0.125
- percolumn_filter_coefficients: bfloat16 [4, 2048], P(None, 'tp'), may hold values from -3 to 3
- switch_tiled_matrices: bfloat16 [2, 2, 32, 64, 64], P(None, None, 'tp'), may hold values from -0.75 to 0.75
- prior_fading_odds: float32 [2, 2048], P(None, 'tp'), may hold values from 2.7 to 17
- speed_factors: float32 [2, 8192], P(None, 'sp'), may hold values from 0.4 to 2.5, as said below
- extra_fading_amounts: float32 [2, 8192], P(None, 'sp'), may hold values from -1.39 to 0, as said below
- averaging_cluster_matrices: bfloat16 [8, 128, 128], P('tp'), may hold values from -0.5 to 0.5
- averaging_feature_factor: bfloat16 [1024], P('tp'), may hold values from 0.099609375 to 1.8984375
- recursive_final_matrix: bfloat16 [2048, 2048], P('tp'), may hold values from -0.25 to 0.25
- averaging_final_matrix: bfloat16 [1024, 2048], P('tp'), may hold values from -0.1875 to 0.1875
Outputs:
- mixed: bfloat16 [8192, 2048], P(('sp', 'tp'))
Inputs may be any that keep to these rules, and one draw needn't show every extreme that they name: `speed_factors`: constant over each aligned block of 512 positions. `extra_fading_amounts`: each row has at most two nonzero entries.
All inputs are finite; a program needn't handle non-finite values.
Results may differ from a plain program's by a relative error of at most 0.017.
Values may be sent and summed in bfloat16 or wider, within the bound.
A program may use at most 128 MiB of HBM per device.

v0:
```python
import jax
import jax.numpy as jnp
from jax import lax
from jax.sharding import PartitionSpec as P

FADING_FACTOR = 8.0
epsilon = 1e-06
span_rows = 16


def padded(block, sides, width):
    for axis, dim in sides:
        count = lax.axis_size(axis)
        forward = [(i, i + 1) for i in range(count - 1)]
        backward = [(target, source) for source, target in forward]
        low = lax.ppermute(
            lax.slice_in_dim(block, block.shape[dim] - width, None, axis=dim), axis, forward
        )
        high = lax.ppermute(lax.slice_in_dim(block, 0, width, axis=dim), axis, backward)
        block = jnp.concatenate([low, block, high], axis=dim)
    return block


def combine(earlier, later):
    return (earlier[0] * later[0], later[0] * earlier[1] + later[1])


def product(left, right):
    return jnp.dot(left, right, preferred_element_type=jnp.float32)


def block_chain(log_keep, drive, backward):
    length, width = log_keep.shape
    count = length // span_rows
    logs = log_keep.reshape(count, span_rows, width)
    sources = drive.reshape(count, span_rows, width)
    running = jnp.cumsum(logs, axis=1)
    place = jnp.arange(span_rows, dtype=jnp.int32)
    if backward:
        running = running[:, -1:] - running + logs
        inside = place[None, :] >= place[:, None]
    else:
        inside = place[None, :] <= place[:, None]
    inside = inside[None, :, :, None]
    spread = running[:, :, None, :] - running[:, None, :, :]
    weights = jnp.where(inside, jnp.exp(jnp.where(inside, spread, 0.0)), 0.0)
    within = jnp.einsum("btsc,bsc->btc", weights, sources)
    decay = jnp.exp(running)
    ones = jnp.ones((1, width), jnp.float32)
    zeros = jnp.zeros((1, width), jnp.float32)
    if backward:
        ends = (decay[:, 0], within[:, 0])
        total_keep, total_state = lax.associative_scan(combine, ends, axis=0, reverse=True)
        prior_keep = jnp.concatenate([total_keep[1:], ones], axis=0)
        prior_state = jnp.concatenate([total_state[1:], zeros], axis=0)
    else:
        ends = (decay[:, -1], within[:, -1])
        total_keep, total_state = lax.associative_scan(combine, ends, axis=0)
        prior_keep = jnp.concatenate([ones, total_keep[:-1]], axis=0)
        prior_state = jnp.concatenate([zeros, total_state[:-1]], axis=0)
    keep_all = decay * prior_keep[:, None]
    local_all = within + decay * prior_state[:, None]
    return (keep_all.reshape(length, width), local_all.reshape(length, width))


def local(
    incoming_activity,
    entry_standardize_factor,
    recursive_entry_matrix,
    final_switch_matrix,
    averaging_entry_matrix,
    percolumn_filter_coefficients,
    switch_tiled_matrices,
    prior_fading_odds,
    speed_factors,
    extra_fading_amounts,
    averaging_cluster_matrices,
    averaging_feature_factor,
    recursive_final_matrix,
    averaging_final_matrix,
):
    state_width = recursive_entry_matrix.shape[1]
    pool_width = averaging_entry_matrix.shape[1]
    gain = entry_standardize_factor.astype(jnp.float32)
    values = lax.all_gather(incoming_activity, "tp", axis=0, tiled=True).astype(jnp.float32)
    scaled = values * lax.rsqrt(jnp.mean(values * values, axis=1, keepdims=True) + epsilon)
    normed = (scaled * gain).astype(jnp.bfloat16)
    projected = jnp.concatenate(
        [
            product(normed, weight).astype(jnp.bfloat16)
            for weight in (recursive_entry_matrix, final_switch_matrix, averaging_entry_matrix)
        ],
        axis=1,
    )
    length = projected.shape[0]
    state_input = projected[:, :state_width]
    gate_input = projected[:, state_width : 2 * state_width]
    pool_input = projected[:, 2 * state_width :]
    conv_rows = padded(state_input, (("sp", 0),), 2).astype(jnp.float32)
    filtered = percolumn_filter_coefficients[0].astype(jnp.float32) * conv_rows[0:length]
    for shift in range(1, percolumn_filter_coefficients.shape[0]):
        filtered = (
            filtered
            + percolumn_filter_coefficients[shift].astype(jnp.float32)
            * conv_rows[shift : shift + length]
        )
    filtered = filtered.astype(jnp.bfloat16)
    filtered_wide = filtered.astype(jnp.float32)
    blocks_here = switch_tiled_matrices.shape[2]
    block_width = switch_tiled_matrices.shape[3]
    gate_sums = jnp.einsum(
        "tbi,dqbij->tdqbj",
        filtered.reshape(length, blocks_here, block_width),
        switch_tiled_matrices,
        preferred_element_type=jnp.float32,
    ).reshape(length, 2, 2, state_width)
    remember_switch = jax.nn.sigmoid(gate_sums[:, :, 0])
    inlet = jax.nn.sigmoid(gate_sums[:, :, 1])
    fading_speed = jax.nn.softplus(-prior_fading_odds)
    logarithmic_persistence = (
        -FADING_FACTOR
        * jnp.transpose(speed_factors)[:, :, None]
        * remember_switch
        * fading_speed[None]
        + jnp.transpose(extra_fading_amounts)[:, :, None]
    )
    drive = jnp.sqrt(-jnp.expm1(2.0 * logarithmic_persistence)) * inlet * filtered_wide[:, None, :]
    forward_keep, forward_local = block_chain(logarithmic_persistence[:, 0], drive[:, 0], False)
    backward_keep, backward_local = block_chain(logarithmic_persistence[:, 1], drive[:, 1], True)
    zeros = jnp.zeros((state_width,), jnp.float32)
    summary = jnp.stack([forward_keep[-1], forward_local[-1], backward_keep[0], backward_local[0]])[
        None
    ]
    totals = lax.all_gather(summary, "sp", axis=0, tiled=True)
    place = lax.axis_index("sp")
    forward_all = lax.associative_scan(combine, (totals[:, 0], totals[:, 1]), axis=0)
    backward_all = lax.associative_scan(combine, (totals[:, 2], totals[:, 3]), axis=0, reverse=True)
    forward_before = jnp.concatenate([zeros[None], forward_all[1]], axis=0)
    backward_after = jnp.concatenate([backward_all[1], zeros[None]], axis=0)
    forward_carry = lax.dynamic_index_in_dim(forward_before, place, 0, keepdims=False)
    backward_carry = lax.dynamic_index_in_dim(backward_after, place + 1, 0, keepdims=False)
    state_sum = (
        forward_local
        + forward_keep * forward_carry[None]
        + backward_local
        + backward_keep * backward_carry[None]
    )
    state_mix = (jax.nn.gelu(gate_input.astype(jnp.float32)) * state_sum).astype(jnp.bfloat16)
    pool_rows = padded(pool_input, (("sp", 0),), 8).astype(jnp.float32)
    spans = []
    level = pool_rows
    for step in range(4):
        shift = 1 << step
        level = level[:-shift] + level[shift:]
        spans.append(level)
    group_width = averaging_cluster_matrices.shape[1]
    local_groups = pool_width // group_width
    group_index = (
        lax.axis_index("tp") * local_groups + jnp.arange(pool_width, dtype=jnp.int32) // group_width
    )
    window_code = group_index % 4
    position = lax.axis_index("sp") * length + jnp.arange(length, dtype=jnp.int32)
    total_length = length * lax.axis_size("sp")
    window_sum = jnp.zeros((length, pool_width), jnp.float32)
    counted = jnp.ones((length, pool_width), jnp.float32)
    for code in range(4):
        half = 1 << code
        begin = 8 - half
        chosen = (window_code == code)[None, :]
        window_count = (
            jnp.minimum(position + half, total_length) - jnp.maximum(position - half, 0)
        ).astype(jnp.float32)[:, None]
        window_sum = jnp.where(chosen, spans[code][begin : begin + length], window_sum)
        counted = jnp.where(chosen, window_count, counted)
    pooled = (window_sum / counted - pool_rows[8 : 8 + length]).astype(jnp.bfloat16)
    grouped = jnp.einsum(
        "tgi,gij->tgj",
        pooled.reshape(length, local_groups, group_width),
        averaging_cluster_matrices,
        preferred_element_type=jnp.float32,
    ).reshape(length, pool_width)
    pool_mix = (grouped * averaging_feature_factor.astype(jnp.float32)).astype(jnp.bfloat16)
    return lax.psum_scatter(
        (
            product(state_mix, recursive_final_matrix) + product(pool_mix, averaging_final_matrix)
        ).astype(jnp.bfloat16),
        "tp",
        scatter_dimension=0,
        tiled=True,
    )


def solution(mesh):
    in_specs = (
        P(("sp", "tp"), None),
        P(),
        P(None, "tp"),
        P(None, "tp"),
        P(None, "tp"),
        P(None, "tp"),
        P(None, None, "tp", None, None),
        P(None, "tp"),
        P(None, "sp"),
        P(None, "sp"),
        P("tp", None, None),
        P("tp"),
        P("tp", None),
        P("tp", None),
    )
    out_specs = P(("sp", "tp"), None)
    return jax.shard_map(local, mesh=mesh, in_specs=in_specs, out_specs=out_specs, check_vma=False)
```

profile of v0, /device:TPU:0, one launch (start us, length us, event | category | flops | bytes accessed | tf_op | source)
XLA Modules:
  0.0 251.2 jit_solution(8073936475268317214)
XLA Ops:
  6.6 0.7 all-gather.4.cloned.1.call-update
  7.3 0.7 convert_element_type.101
  8.0 0.7 convert_element_type.85
  8.7 1.6 copy.54
  10.5 34.2 %all-gather.4.cloned.1.call-done = bf16[512,2048]{1,0:T(8,128)(2,1)} async-done(((bf16[256,2048]{1,0:T(8,128)(2,1)}), bf16[512,2048]{1,0:T(8,128)(2,1)}) %all-gather.4.cloned.1.call-update) | async-done | bytes 2097168 | tf_op jit(solution)/shard_map/all_gather | solution.py:85
  44.7 2.2 fusion
  47.0 4.7 %convolution_convert_fusion = bf16[512,1024]{1,0:T(8,128)(2,1)S(1)} fusion(bf16[2048,1024]{1,0:T(8,128)(2,1)} %param.16, bf16[512,2048]{1,0:T(8,128)(2,1)S(1)} %copy-done.9, f32[2048]{0:T(1024)S(1)} %convert_element_type.85, f32[512]{0:T(512)S(1)} %add_rsqrt_fusion), kind=kOutput, calls=%fused_computation.44 | convolution fusion | flops 2152202240 | bytes 7350272 | tf_op jit(solution)/shard_map/dot_general | solution.py:29
  51.8 1.6 collective-permute-start
  53.3 1.3 collective-permute-start.1
  54.6 1.3 convolution_convert_fusion.2
  56.0 4.5 %collective-permute-start.2 = (bf16[8,512]{1,0:T(8,128)(2,1)S(1)}, bf16[8,512]{1,0:T(8,128)(2,1)S(1)}, u32[]{:S(2)}, u32[]{:S(2)}) collective-permute-start(bf16[8,512]{1,0:T(8,128)(2,1)S(1)} %get-tuple-element.24), channel_id=1, source_target_pairs={{0,2},{2,4},{4,6},{6,8},{8,10},{10,12},{12,14},{14,16},{16,18},{18... | collective-permute-start | bytes 24584 | tf_op jit(solution)/shard_map/ppermute | solution.py:16
  60.4 1.3 collective-permute-start.3
  61.8 0.3 maximum_convert_fusion
  62.1 2.6 %fusion.71 = (f32[512,1024]{1,0:T(8,128)}, bf16[512,1024]{1,0:T(8,128)(2,1)}) fusion(f32[516,1024]{1,0:T(8,128)S(1)} %maximum_convert_fusion, f32[1024]{0:T(1024)S(1)} %bitcast.154, f32[1024]{0:T(1024)S(1)} %bitcast.155, f32[1024]{0:T(1024)S(1)} %bitcast.153, f32[1024]{0:T(1024)S(1)} %bitcast.152), kind=kLoop, calls=%fused_computation.227 | loop fusion | flops 4718592 | bytes 11550720 | tf_op jit(solution)/shard_map/convert_element_type | solution.py:108
  64.7 2.8 %copy.53 = bf16[512,1024]{0,1:T(8,128)(2,1)} copy(bf16[512,1024]{1,0:T(8,128)(2,1)} %get-tuple-element.8) | data formatting | bytes 2097152 | tf_op jit(solution)/shard_map/convert_element_type | solution.py:107
  67.4 2.5 fusion.96
  69.9 1.8 copy.55
  71.7 4.2 %fusion.74 = (f32[512,2,1,1024]{0,3,2,1:T(8,128)}, f32[512,2,1,1024]{0,3,2,1:T(8,128)}) fusion(f32[512,2,2,1024]{0,3,2,1:T(8,128)S(1)} %bitcast.122), kind=kLoop, calls=%fused_computation.229 | loop fusion | bytes 16777216 | tf_op jit(solution)/shard_map/slice | solution.py:117
  75.9 5.4 %copy.92 = f32[512,2,1,1024]{3,0,1,2:T(8,128)} copy(f32[512,2,1,1024]{0,3,2,1:T(8,128)} %get-tuple-element.12) | data formatting | bytes 8388608
  81.3 5.4 %copy.93 = f32[512,2,1,1024]{3,0,1,2:T(8,128)} copy(f32[512,2,1,1024]{0,3,2,1:T(8,128)} %get-tuple-element.13) | data formatting | bytes 8388608
  86.7 7.3 %fusion.3 = (f32[512,2,1024]{2,0,1:T(8,128)S(1)}, f32[512,2,1024]{2,0,1:T(8,128)S(1)}) fusion(f32[512,2,1,1024]{3,0,1,2:T(8,128)} %copy.93, f32[512,1024]{1,0:T(8,128)} %get-tuple-element.7, f32[512,2]{0,1:T(2,128)S(1)} %bitcast.158, f32[2,1024]{1,0:T(2,128)S(1)} %compare_select_fusion, f32[512,2,1,1024]{3,0,1,2:T(8,128)} %copy.92, ...), kind=kLoop, calls=%fused_computation.8 | loop fusion | flops 13631488 | bytes 18890752 | tf_op jit(solution)/shard_map/mul | solution.py:127
  94.0 3.3 %fusion.75 = (f32[512,1,1024]{2,0,1:T(8,128)}, f32[512,1,1024]{2,0,1:T(8,128)S(1)}, f32[512,1,1024]{2,0,1:T(8,128)}, f32[512,1,1024]{2,0,1:T(8,128)}) fusion(f32[512,2,1024]{2,0,1:T(8,128)S(1)} %get-tuple-element.6, f32[512,2,1024]{2,0,1:T(8,128)S(1)} %get-tuple-element.5), kind=kLoop, calls=%fused_computation.230 | loop fusion | bytes 16777216 | tf_op jit(solution)/shard_map/slice | solution.py:128
  97.3 0.6 copy-done.1
  97.9 1.3 fusion.20
  99.2 3.6 %fusion.73 = (f32[32,16,1024]{2,0,1:T(8,128)S(1)}, f32[32,16,1024]{2,0,1:T(8,128)}, f32[32,16,1024]{2,0,1:T(8,128)}) fusion(f32[32,16,1024]{2,1,0:T(8,128)S(1)} %bitcast.124, f32[32,16,1024]{2,0,1:T(8,128)S(1)} %fusion.20, f32[32,1024]{1,0:T(8,128)S(1)} %slice_bitcast_fusion.2), kind=kLoop, calls=%fused_computation.228 | loop fusion | flops 1048576 | bytes 10616832 | tf_op jit(solution)/shard_map/exp | solution.py:48
  102.9 3.0 %copy.66 = f32[32,16,1024]{2,1,0:T(8,128)S(1)} copy(f32[32,16,1024]{2,0,1:T(8,128)} %get-tuple-element.10) | data formatting | bytes 4194304 | tf_op jit(solution)/shard_map/add | solution.py:40
  105.9 12.3 %multiply_reduce_fusion = f32[32,1024,16]{1,2,0:T(8,128)S(1)} fusion(f32[32,1024,16]{1,2,0:T(8,128)S(1)} %bitcast.139, f32[32,16,1024]{2,1,0:T(8,128)S(1)} %copy.66, pred[16,16]{1,0:T(8,128)(4,1)S(1)} %iota_compare_fusion), kind=kLoop, calls=%fused_computation | loop fusion | flops 41418752 | bytes 6291712
  118.2 1.2 copy.121
  119.6 0.2 slice.739
  119.8 0.2 slice.741
  119.9 0.2 slice.770
  120.1 0.2 slice.772
  120.9 4.3 %fusion.95 = (f32[32,16,1024]{2,0,1:T(8,128)S(1)}, f32[32,16,1024]{2,0,1:T(8,128)}) fusion(f32[32,16,1024]{2,1,0:T(8,128)} %bitcast.125), kind=kOutput, calls=%fused_computation.250 | output fusion | flops 7864320 | bytes 6291456 | tf_op jit(solution)/shard_map/jit(cumsum)/reduce_window_sum | solution.py:37
  125.3 3.0 %copy.59 = f32[32,16,1024]{2,1,0:T(8,128)S(1)} copy(f32[32,16,1024]{2,0,1:T(8,128)} %get-tuple-element.97) | data formatting | bytes 4194304 | tf_op jit(solution)/shard_map/jit(cumsum)/reduce_window_sum | solution.py:37
  128.3 12.1 %multiply_reduce_fusion.1 = f32[32,1024,16]{1,2,0:T(8,128)S(1)} fusion(f32[32,1024,16]{1,2,0:T(8,128)S(1)} %bitcast.138, f32[32,16,1024]{2,1,0:T(8,128)S(1)} %copy.59, pred[16,16]{1,0:T(8,128)(4,1)S(1)} %iota_compare_fusion.1), kind=kLoop, calls=%fused_computation.1 | loop fusion | flops 41418752 | bytes 6291712
  140.5 1.2 copy.122
  142.5 4.1 %copy.64 = f32[32,16,1024]{2,1,0:T(8,128)} copy(f32[32,16,1024]{2,0,1:T(8,128)} %get-tuple-element.11) | data formatting | bytes 4194304 | tf_op jit(solution)/shard_map/sub | solution.py:40
  146.6 0.2 slice.761
  146.8 0.2 slice.792
  147.8 0.5 slice.794
  148.2 3.7 %multiply_add_fusion = f32[32,16,1024]{2,0,1:T(8,128)S(1)} fusion(f32[32,1024]{1,0:T(8,128)S(1)} %concatenate.110, f32[32,1024,16]{1,2,0:T(8,128)} %copy-done.3, f32[32,16,1024]{2,0,1:T(8,128)} %get-tuple-element.10), kind=kLoop, calls=%fused_computation.39 | loop fusion | flops 1048576 | bytes 6422528 | tf_op jit(solution)/shard_map/add | solution.py:62
  152.0 1.2 copy.68
  153.2 1.4 copy-done.6
  154.6 0.2 slice.763
  154.9 2.8 %bitcast_multiply_fusion.2 = f32[512,1024]{1,0:T(8,128)S(1)} fusion(f32[32,16,1024]{2,1,0:T(8,128)} %copy.64, f32[32,1024]{1,0:T(8,128)S(1)} %concatenate.105, f32[512,2,1024]{2,0,1:T(8,128)} %copy-done.1), kind=kLoop, calls=%fused_computation.32 | loop fusion | flops 1048576 | bytes 6422528 | tf_op jit(solution)/shard_map/mul | solution.py:61
  157.7 1.4 copy-done.5
  159.9 3.7 %broadcast_multiply_fusion = (f32[32,16,1024]{2,0,1:T(8,128)S(1)}, f32[32,16,1024]{2,0,1:T(8,128)S(1)}) fusion(f32[32,1024]{1,0:T(8,128)S(1)} %concatenate.100, f32[32,16,1024]{2,0,1:T(8,128)} %get-tuple-element.97, f32[32,1024]{1,0:T(8,128)S(1)} %concatenate.95, f32[32,1024,16]{1,2,0:T(8,128)} %copy-done.4), kind=kLoop, calls=%fused_computation.62 | loop fusion | flops 1572864 | bytes 8650752 | tf_op jit(solution)/shard_map/mul | solution.py:61
  163.6 1.2 copy.62
  164.9 1.2 copy.61
  166.2 1.4 copy-done.8
  167.6 24.5 %all-gather.1 = f32[16,4,1024]{2,1,0:T(4,128)S(1)} all-gather(f32[1,4,1024]{2,1,0:T(4,128)S(1)} %maximum_bitcast_fusion), channel_id=2, replica_groups=mesh['sp'=16,'tp'=2] {'sp'}, dimensions={0}, use_global_device_ids=true | all-gather | bytes 278528 | tf_op jit(solution)/shard_map/all_gather | solution.py:134
  192.1 0.2 fusion.80
  193.1 0.4 slice.835
  193.8 0.2 slice.832
  194.6 0.2 slice.861
  194.8 0.2 slice.830
  195.3 0.2 rev.2
  195.6 13.8 %fusion.28 = f32[512,2048]{1,0:T(8,128)} fusion(bf16[1024,2048]{1,0:T(8,128)(2,1)} %param.26, f32[512,1024]{1,0:T(8,128)} %copy-done.5, f32[512,1024]{1,0:T(8,128)} %bitcast.133, f32[512,1024]{1,0:T(8,128)} %bitcast.137, f32[512,1024]{1,0:T(8,128)} %bitcast.135, bf16[2048,1024]{1,0:T(8,128)(2,1)} %param.17, f32[1024]{0:T(1024)S(1)} %bitcast.157, ...), kind=kOutput, calls=%fused_computation.63 | convolution fusion | flops 4308074496 | bytes 23087104 | tf_op jit(solution)/shard_map/dot_general | solution.py:29
  210.0 0.3 fusion.77
  210.3 0.6 copy-done.19
  210.9 1.3 fusion.29
  212.3 0.8 copy-done.2
  213.1 2.6 %add_convert_fusion = bf16[512,2048]{1,0:T(8,128)(2,1)} fusion(f32[512,2048]{1,0:T(8,128)S(1)} %copy-done.2, bf16[512,512]{0,1:T(8,128)(2,1)S(1)} %fusion.27, bf16[512,2048]{1,0:T(8,128)(2,1)S(1)} %copy-done), kind=kOutput, calls=%fused_computation.12 | convolution fusion | flops 1075838976 | bytes 8912896 | tf_op jit(solution)/shard_map/dot_general | solution.py:29
  215.7 28.4 %reduce-scatter.2.cloned.1.call-done = bf16[256,2048]{1,0:T(8,128)(2,1)} async-done(((bf16[512,2048]{1,0:T(8,128)(2,1)}), bf16[256,2048]{1,0:T(8,128)(2,1)}) %reduce-scatter.2.cloned.1.call-update) | async-done | bytes 1048592 | tf_op jit(solution)/shard_map/reduce_scatter | solution.py:183
  (297 shorter events, 5.5 us)
Async XLA Ops:
  6.5 205.8 %copy-start = (bf16[512,2048]{1,0:T(8,128)(2,1)S(1)}, bf16[512,2048]{1,0:T(8,128)(2,1)}, u32[]{:S(2)}) copy-start(bf16[512,2048]{1,0:T(8,128)(2,1)} %param.27) | copy-start | bytes 6291460
  6.5 3.9 %copy-start.16 = (f32[2,512]{1,0:T(2,128)S(1)}, f32[2,512]{1,0:T(2,128)}, u32[]{:S(2)}) copy-start(f32[2,512]{1,0:T(2,128)} %param.22) | copy-start | bytes 12292
  6.5 3.9 %copy-start.15 = (f32[2,1024]{1,0:T(2,128)S(1)}, f32[2,1024]{1,0:T(2,128)}, u32[]{:S(2)}) copy-start(f32[2,1024]{1,0:T(2,128)} %param.21) | copy-start | bytes 24580
  6.5 3.9 %copy-start.14 = (bf16[4,1024]{1,0:T(4,128)(2,1)S(1)}, bf16[4,1024]{1,0:T(4,128)(2,1)}, u32[]{:S(2)}) copy-start(bf16[4,1024]{1,0:T(4,128)(2,1)} %param.19) | copy-start | bytes 24580
  6.5 38.2 %all-gather.4.cloned.1.call-start = ((), (), s32[]{:S(2)}) async-start(), calls=%async_computation.1 | async-start | bytes 3145728 | tf_op jit(solution)/shard_map/all_gather | solution.py:85
  7.3 236.9 %reduce-scatter.2.cloned.1.call-start = ((), (), s32[]{:S(2)}) async-start(), calls=%async_computation.2 | async-start | bytes 3145728 | tf_op jit(solution)/shard_map/reduce_scatter | solution.py:183
  44.7 2.2 copy-start.9
  47.0 7.6 %copy-start.18 = (bf16[2048,512]{1,0:T(8,128)(2,1)S(1)}, bf16[2048,512]{1,0:T(8,128)(2,1)}, u32[]{:S(2)}) copy-start(bf16[2048,512]{1,0:T(8,128)(2,1)} %param.18) | copy-start | bytes 6291460
  51.8 10.0 %collective-permute-start = (bf16[2,1024]{1,0:T(2,128)(2,1)S(1)}, bf16[2,1024]{1,0:T(2,128)(2,1)S(1)}, u32[]{:S(2)}, u32[]{:S(2)}) collective-permute-start(bf16[2,1024]{1,0:T(2,128)(2,1)S(1)} %get-tuple-element.22), channel_id=1, source_target_pairs={{0,2},{2,4},{4,6},{6,8},{8,10},{10,12},{12,14},{14,16},{16,18},{18... | collective-permute-start | bytes 12296 | tf_op jit(solution)/shard_map/ppermute | solution.py:16
  53.3 8.4 %collective-permute-start.1 = (bf16[2,1024]{1,0:T(2,128)(2,1)S(1)}, bf16[2,1024]{1,0:T(2,128)(2,1)S(1)}, u32[]{:S(2)}, u32[]{:S(2)}) collective-permute-start(bf16[2,1024]{1,0:T(2,128)(2,1)S(1)} %get-tuple-element.23), channel_id=1, source_target_pairs={{2,0},{4,2},{6,4},{8,6},{10,8},{12,10},{14,12},{16,14},{18,16},{20... | collective-permute-start | bytes 12296 | tf_op jit(solution)/shard_map/ppermute | solution.py:19
  55.9 6.1 %copy-start.12 = (bf16[512,512]{1,0:T(8,128)(2,1)}, bf16[512,512]{1,0:T(8,128)(2,1)S(1)}, u32[]{:S(2)}) copy-start(bf16[512,512]{1,0:T(8,128)(2,1)S(1)} %convolution_convert_fusion.2) | copy-start | bytes 1572868
  56.0 153.4 %collective-permute-start.2 = (bf16[8,512]{1,0:T(8,128)(2,1)S(1)}, bf16[8,512]{1,0:T(8,128)(2,1)S(1)}, u32[]{:S(2)}, u32[]{:S(2)}) collective-permute-start(bf16[8,512]{1,0:T(8,128)(2,1)S(1)} %get-tuple-element.24), channel_id=1, source_target_pairs={{0,2},{2,4},{4,6},{6,8},{8,10},{10,12},{12,14},{14,16},{16,18},{18... | collective-permute-start | bytes 24584 | tf_op jit(solution)/shard_map/ppermute | solution.py:16
  60.4 148.9 %collective-permute-start.3 = (bf16[8,512]{1,0:T(8,128)(2,1)S(1)}, bf16[8,512]{1,0:T(8,128)(2,1)S(1)}, u32[]{:S(2)}, u32[]{:S(2)}) collective-permute-start(bf16[8,512]{1,0:T(8,128)(2,1)S(1)} %get-tuple-element.25), channel_id=1, source_target_pairs={{2,0},{4,2},{6,4},{8,6},{10,8},{12,10},{14,12},{16,14},{18,16},{20... | collective-permute-start | bytes 24584 | tf_op jit(solution)/shard_map/ppermute | solution.py:19
  81.3 5.4 %copy-start.17 = (f32[2,512]{1,0:T(2,128)S(1)}, f32[2,512]{1,0:T(2,128)}, u32[]{:S(2)}) copy-start(f32[2,512]{1,0:T(2,128)} %param.23) | copy-start | bytes 12292
  94.0 3.9 %copy-start.1 = (f32[512,2,1024]{2,0,1:T(8,128)}, f32[512,2,1024]{2,0,1:T(8,128)S(1)}, u32[]{:S(2)}) copy-start(f32[512,2,1024]{2,0,1:T(8,128)S(1)} %get-tuple-element.6) | copy-start | bytes 12582916
  102.9 3.0 %copy-start.11 = (f32[512,1,1024]{2,0,1:T(8,128)S(1)}, f32[512,1,1024]{2,0,1:T(8,128)}, u32[]{:S(2)}) copy-start(f32[512,1,1024]{2,0,1:T(8,128)} %get-tuple-element.98) | copy-start | bytes 6291460
  118.2 1.3 copy-start.3
  125.3 3.0 %copy-start.10 = (f32[512,1,1024]{2,0,1:T(8,128)S(1)}, f32[512,1,1024]{2,0,1:T(8,128)}, u32[]{:S(2)}) copy-start(f32[512,1,1024]{2,0,1:T(8,128)} %get-tuple-element.99) | copy-start | bytes 6291460
  140.4 1.3 copy-start.4
  153.2 1.4 copy-start.6
  157.7 1.4 copy-start.5
  164.9 1.3 copy-start.7
  166.2 1.4 copy-start.8
  195.6 13.8 %copy-start.13 = (bf16[512,512]{1,0:T(8,128)(2,1)S(1)}, bf16[512,512]{1,0:T(8,128)(2,1)}, u32[]{:S(2)}) copy-start(bf16[512,512]{1,0:T(8,128)(2,1)} %copy-done.12) | copy-start | bytes 1572868
  210.0 0.9 copy-start.19
  210.9 2.2 copy-start.2
Sparse Core Ops, SparseCore 0:
  8.9 35.8 all-gather.3
  215.9 28.2 reduce-scatter.1
where the time goes:
time: 256 us; the launch traced here: 251 us
  waiting for transfers between devices  63.3 us (25%)
  other arithmetic  59.5 us (23%)
  local copies, waits for them, and re-layouts  53.5 us (21%)
  matrix products  26.1 us (10%)
  blocking collectives  24.5 us (10%)
  between operations  15.5 us (6%)
  starting transfers between devices  8.69 us (3%)
    all_gather x1, waiting for transfers between devices, local(): lax.all_gather(incoming_activity, 'tp', axis=0, tiled=True)  34.2 us
    reduce_scatter x1, waiting for transfers between devices, local(): lax.psum_scatter((product(state_mix, recursive_final_matrix) + product(po...  28.4 us
    all_gather x1, blocking collectives, local(): totals = lax.all_gather(summary, 'sp', axis=0, tiled=True)  24.5 us
    unnamed x3, other arithmetic  24.5 us
    dot_general x4, matrix products, product(): return jnp.dot(left, right, preferred_element_type=jnp.float32)  22.4 us
    unnamed x51, local copies, waits for them, and re-layouts  18.9 us
    mul x1, other arithmetic, local(): jnp.sqrt(-jnp.expm1(2.0 * logarithmic_persistence)) * inlet  7.26 us
    mul x2, other arithmetic, block_chain(): keep_all = decay * prior_keep[:, None]  6.51 us
  transfers between devices with their start and end apart: 6, of which 2 were waited for; matrix products, arithmetic and copies ran while one was open for 48% of the time, Pallas kernels for 0%

commit v1 on v0

--- a/solution.py
+++ b/solution.py
@@ -6,6 +6,27 @@
 FADING_FACTOR = 8.0
 epsilon = 1e-06
 span_rows = 16
+
+
+def gather_around(x, axis, dim):
+    length, index, rows = (lax.axis_size(axis), lax.axis_index(axis), x.shape[dim])
+    right = [(i, (i + 1) % length) for i in range(length)]
+    downward = [(i, (i - 1) % length) for i in range(length)]
+    out = jnp.zeros((*x.shape[:dim], length * rows, *x.shape[dim + 1 :]), x.dtype)
+    out = lax.dynamic_update_slice_in_dim(out, x, index * rows, axis=dim)
+    from_left = from_right = x
+    half = length // 2
+    for lap in range(1, half + 1):
+        from_left = lax.ppermute(from_left, axis, right)
+        out = lax.dynamic_update_slice_in_dim(
+            out, from_left, (index - lap) % length * rows, axis=dim
+        )
+        if lap < length - half:
+            from_right = lax.ppermute(from_right, axis, downward)
+            out = lax.dynamic_update_slice_in_dim(
+                out, from_right, (index + lap) % length * rows, axis=dim
+            )
+    return out
 
 
 def padded(block, sides, width):
@@ -131,7 +152,7 @@
     summary = jnp.stack([forward_keep[-1], forward_local[-1], backward_keep[0], backward_local[0]])[
         None
     ]
-    totals = lax.all_gather(summary, "sp", axis=0, tiled=True)
+    totals = gather_around(summary, "sp", 0)
     place = lax.axis_index("sp")
     forward_all = lax.associative_scan(combine, (totals[:, 0], totals[:, 1]), axis=0)
     backward_all = lax.associative_scan(combine, (totals[:, 2], totals[:, 3]), axis=0, reverse=True)

time: 256 us -> 278 us (1.086)
  starting transfers between devices: 8.69 us -> 39.7 us
  blocking collectives: 24.5 us -> 0 us
  waiting for transfers between devices: 63.3 us -> 75.3 us
  matrix products: 26.1 us -> 29.1 us
    ppermute x0 -> x15, starting transfers between devices: none -> 32.7 us  [the longest x7 30 us: gather_around(): from_right = lax.ppermute(from_right, axis, downward)]
    all_gather x1 -> x0, blocking collectives: 24.5 us -> none  [local(): totals = lax.all_gather(summary, 'sp', axis=0, tiled=True)]
    ppermute x0 -> x15, waiting for transfers between devices: none -> 9.6 us  [the longest x7 5.01 us: gather_around(): from_right = lax.ppermute(from_right, axis, downward)]
    dot_general x4, matrix products: 22.4 us -> 25.4 us  [product(): return jnp.dot(left, right, preferred_element_type=jnp.float32)]
    unnamed x51 -> x45, local copies, waits for them, and re-layouts: 18.9 us -> 17.4 us
    unnamed x3 -> x2, other arithmetic: 24.5 us -> 24.5 us
  transfers between devices with their start and end apart: 6 -> 21, of which waited for: 2 -> 15; matrix products, arithmetic and copies ran while one was open for 48% -> 3% of each run, Pallas kernels for 0% -> 0%
where the time goes in v1:
time: 278 us; the launch traced here: 273 us
  waiting for transfers between devices  75.3 us (27%)
  other arithmetic  58.9 us (21%)
  local copies, waits for them, and re-layouts  54.1 us (19%)
  starting transfers between devices  39.7 us (14%)
  matrix products  29.1 us (10%)
  between operations  16 us (6%)
    all_gather x1, waiting for transfers between devices, local(): lax.all_gather(incoming_activity, 'tp', axis=0, tiled=True)  34.8 us
    ppermute x7, starting transfers between devices, gather_around(): from_right = lax.ppermute(from_right, axis, downward)  30 us
    reduce_scatter x1, waiting for transfers between devices, local(): lax.psum_scatter((product(state_mix, recursive_final_matrix) + product(po...  29.2 us
    dot_general x4, matrix products, product(): return jnp.dot(left, right, preferred_element_type=jnp.float32)  25.4 us
    unnamed x2, other arithmetic  24.5 us
    unnamed x45, local copies, waits for them, and re-layouts  17.4 us
    mul x1, other arithmetic, local(): jnp.sqrt(-jnp.expm1(2.0 * logarithmic_persistence)) * inlet  7.26 us
    mul x2, other arithmetic, block_chain(): keep_all = decay * prior_keep[:, None]  6.51 us
  transfers between devices with their start and end apart: 21, of which 15 were waited for; matrix products, arithmetic and copies ran while one was open for 3% of the time, Pallas kernels for 0%

profile of v1, /device:TPU:0, one launch (start us, length us, event | category | flops | bytes accessed | tf_op | source)
XLA Modules:
  0.0 273.1 jit_solution(18295501291454773432)
XLA Ops:
  6.6 0.7 all-gather.2.cloned.1.call-update
  7.4 0.7 convert_element_type.85
  8.1 1.6 copy.52
  9.9 34.8 %all-gather.2.cloned.1.call-done = bf16[512,2048]{1,0:T(8,128)(2,1)} async-done(((bf16[256,2048]{1,0:T(8,128)(2,1)}), bf16[512,2048]{1,0:T(8,128)(2,1)}) %all-gather.2.cloned.1.call-update) | async-done | bytes 2097168 | tf_op jit(solution)/shard_map/all_gather | solution.py:106
  44.7 2.2 fusion
  47.0 4.7 %convolution_convert_fusion = bf16[512,1024]{1,0:T(8,128)(2,1)S(1)} fusion(bf16[2048,1024]{1,0:T(8,128)(2,1)} %param.16, bf16[512,2048]{1,0:T(8,128)(2,1)S(1)} %copy-done.8, f32[2048]{0:T(1024)S(1)} %convert_element_type.85, f32[512]{0:T(512)S(1)} %add_rsqrt_fusion), kind=kOutput, calls=%fused_computation.44 | convolution fusion | flops 2152202240 | bytes 7350272 | tf_op jit(solution)/shard_map/dot_general | solution.py:50
  51.7 1.6 collective-permute-start
  53.3 1.3 collective-permute-start.1
  54.6 2.1 convolution_convert_fusion.2
  56.7 1.1 collective-permute-done.1
  57.8 0.3 maximum_convert_fusion
  58.1 2.6 fusion.71
  60.7 2.4 copy.51
  63.1 2.4 fusion.95
  65.6 1.8 copy.53
  67.4 4.2 %fusion.74 = (f32[512,2,1,1024]{0,3,2,1:T(8,128)}, f32[512,2,1,1024]{0,3,2,1:T(8,128)}) fusion(f32[512,2,2,1024]{0,3,2,1:T(8,128)S(1)} %bitcast.124), kind=kLoop, calls=%fused_computation.229 | loop fusion | bytes 16777216 | tf_op jit(solution)/shard_map/slice | solution.py:138
  71.6 5.4 %copy.108 = f32[512,2,1,1024]{3,0,1,2:T(8,128)} copy(f32[512,2,1,1024]{0,3,2,1:T(8,128)} %get-tuple-element.12) | data formatting | bytes 8388608
  77.0 5.4 %copy.109 = f32[512,2,1,1024]{3,0,1,2:T(8,128)} copy(f32[512,2,1,1024]{0,3,2,1:T(8,128)} %get-tuple-element.13) | data formatting | bytes 8388608
  82.4 7.3 %fusion.3 = (f32[512,2,1024]{2,0,1:T(8,128)S(1)}, f32[512,2,1024]{2,0,1:T(8,128)S(1)}) fusion(f32[512,2,1,1024]{3,0,1,2:T(8,128)} %copy.109, f32[512,1024]{1,0:T(8,128)} %get-tuple-element.7, f32[512,2]{0,1:T(2,128)S(1)} %bitcast.148, f32[2,1024]{1,0:T(2,128)S(1)} %compare_select_fusion, f32[512,2,1,1024]{3,0,1,2:T(8,128)} %copy.108, ...), kind=kLoop, calls=%fused_computation.8 | loop fusion | flops 13631488 | bytes 18890752 | tf_op jit(solution)/shard_map/mul | solution.py:148
  89.7 3.3 %fusion.75 = (f32[512,1,1024]{2,0,1:T(8,128)}, f32[512,1,1024]{2,0,1:T(8,128)S(1)}, f32[512,1,1024]{2,0,1:T(8,128)}, f32[512,1,1024]{2,0,1:T(8,128)}) fusion(f32[512,2,1024]{2,0,1:T(8,128)S(1)} %get-tuple-element.6, f32[512,2,1024]{2,0,1:T(8,128)S(1)} %get-tuple-element.5), kind=kLoop, calls=%fused_computation.230 | loop fusion | bytes 16777216 | tf_op jit(solution)/shard_map/slice | solution.py:149
  92.9 0.6 copy-done.1
  93.6 1.3 fusion.20
  94.9 3.6 %fusion.73 = (f32[32,16,1024]{2,0,1:T(8,128)S(1)}, f32[32,16,1024]{2,0,1:T(8,128)}, f32[32,16,1024]{2,0,1:T(8,128)}) fusion(f32[32,16,1024]{2,1,0:T(8,128)S(1)} %bitcast.126, f32[32,16,1024]{2,0,1:T(8,128)S(1)} %fusion.20, f32[32,1024]{1,0:T(8,128)S(1)} %slice_bitcast_fusion.2), kind=kLoop, calls=%fused_computation.228 | loop fusion | flops 1048576 | bytes 10616832 | tf_op jit(solution)/shard_map/exp | solution.py:69
  98.6 3.0 %copy.64 = f32[32,16,1024]{2,1,0:T(8,128)S(1)} copy(f32[32,16,1024]{2,0,1:T(8,128)} %get-tuple-element.10) | data formatting | bytes 4194304 | tf_op jit(solution)/shard_map/add | solution.py:61
  101.6 12.3 %multiply_reduce_fusion = f32[32,1024,16]{1,2,0:T(8,128)S(1)} fusion(f32[32,1024,16]{1,2,0:T(8,128)S(1)} %bitcast.141, f32[32,16,1024]{2,1,0:T(8,128)S(1)} %copy.64, pred[16,16]{1,0:T(8,128)(4,1)S(1)} %iota_compare_fusion), kind=kLoop, calls=%fused_computation | loop fusion | flops 41418752 | bytes 6291712
  113.9 1.2 copy.135
  116.6 4.3 %fusion.94 = (f32[32,16,1024]{2,0,1:T(8,128)S(1)}, f32[32,16,1024]{2,0,1:T(8,128)}) fusion(f32[32,16,1024]{2,1,0:T(8,128)} %bitcast.127), kind=kOutput, calls=%fused_computation.249 | output fusion | flops 7864320 | bytes 6291456 | tf_op jit(solution)/shard_map/jit(cumsum)/reduce_window_sum | solution.py:58
  121.1 3.0 %copy.57 = f32[32,16,1024]{2,1,0:T(8,128)S(1)} copy(f32[32,16,1024]{2,0,1:T(8,128)} %get-tuple-element.97) | data formatting | bytes 4194304 | tf_op jit(solution)/shard_map/jit(cumsum)/reduce_window_sum | solution.py:58
  124.0 12.1 %multiply_reduce_fusion.1 = f32[32,1024,16]{1,2,0:T(8,128)S(1)} fusion(f32[32,1024,16]{1,2,0:T(8,128)S(1)} %bitcast.140, f32[32,16,1024]{2,1,0:T(8,128)S(1)} %copy.57, pred[16,16]{1,0:T(8,128)(4,1)S(1)} %iota_compare_fusion.1), kind=kLoop, calls=%fused_computation.1 | loop fusion | flops 41418752 | bytes 6291712
  136.2 1.2 copy.136
  138.2 4.1 %copy.62 = f32[32,16,1024]{2,1,0:T(8,128)} copy(f32[32,16,1024]{2,0,1:T(8,128)} %get-tuple-element.11) | data formatting | bytes 4194304 | tf_op jit(solution)/shard_map/sub | solution.py:61
  143.5 0.6 slice.794
  144.2 3.7 %multiply_add_fusion = f32[32,16,1024]{2,0,1:T(8,128)S(1)} fusion(f32[32,1024]{1,0:T(8,128)S(1)} %concatenate.110, f32[32,1024,16]{1,2,0:T(8,128)} %copy-done.2, f32[32,16,1024]{2,0,1:T(8,128)} %get-tuple-element.10), kind=kLoop, calls=%fused_computation.39 | loop fusion | flops 1048576 | bytes 6422528 | tf_op jit(solution)/shard_map/add | solution.py:83
  147.9 1.2 copy.66
  149.1 1.4 copy-done.5
  150.8 2.8 %bitcast_multiply_fusion.2 = f32[512,1024]{1,0:T(8,128)S(1)} fusion(f32[32,16,1024]{2,1,0:T(8,128)} %copy.62, f32[32,1024]{1,0:T(8,128)S(1)} %concatenate.105, f32[512,2,1024]{2,0,1:T(8,128)} %copy-done.1), kind=kLoop, calls=%fused_computation.32 | loop fusion | flops 1048576 | bytes 6422528 | tf_op jit(solution)/shard_map/mul | solution.py:82
  153.6 1.4 copy-done.4
  155.8 3.7 %broadcast_multiply_fusion = (f32[32,16,1024]{2,0,1:T(8,128)S(1)}, f32[32,16,1024]{2,0,1:T(8,128)S(1)}) fusion(f32[32,1024]{1,0:T(8,128)S(1)} %concatenate.100, f32[32,16,1024]{2,0,1:T(8,128)} %get-tuple-element.97, f32[32,1024]{1,0:T(8,128)S(1)} %concatenate.95, f32[32,1024,16]{1,2,0:T(8,128)} %copy-done.3), kind=kLoop, calls=%fused_computation.62 | loop fusion | flops 1572864 | bytes 8650752 | tf_op jit(solution)/shard_map/mul | solution.py:82
  159.5 1.2 copy.60
  160.8 1.2 copy.59
  162.1 1.4 copy-done.7
  163.5 2.4 collective-permute-start.2
  165.9 2.7 %collective-permute-start.17 = (bf16[8,512]{1,0:T(8,128)(2,1)S(1)}, bf16[8,512]{1,0:T(8,128)(2,1)S(1)}, u32[]{:S(2)}, u32[]{:S(2)}) collective-permute-start(bf16[8,512]{1,0:T(8,128)(2,1)S(1)} %get-tuple-element.24), channel_id=1, source_target_pairs={{0,2},{2,4},{4,6},{6,8},{8,10},{10,12},{12,14},{14,16},{16,18},{18... | collective-permute-start | bytes 24584 | tf_op jit(solution)/shard_map/ppermute | solution.py:37
  168.6 1.3 collective-permute-start.18
  170.2 3.5 %collective-permute-start.3 = (f32[1,4,1024]{2,1,0:T(4,128)S(1)}, f32[1,4,1024]{2,1,0:T(4,128)S(1)}, u32[]{:S(2)}, u32[]{:S(2)}) collective-permute-start(f32[1,4,1024]{2,1,0:T(4,128)S(1)} %maximum_bitcast_fusion), channel_id=1, source_target_pairs={{0,30},{2,0},{4,2},{6,4},{8,6},{10,8},{12,10},{14,12},{16,14},{18,... | collective-permute-start | bytes 49160 | tf_op jit(solution)/shard_map/ppermute | solution.py:25
  174.1 1.0 collective-permute-done.3
  175.1 4.4 %collective-permute-start.5 = (f32[1,4,1024]{2,1,0:T(4,128)S(1)}, f32[1,4,1024]{2,1,0:T(4,128)S(1)}, u32[]{:S(2)}, u32[]{:S(2)}) collective-permute-start(f32[1,4,1024]{2,1,0:T(4,128)S(1)} %collective-permute-done.3), channel_id=1, source_target_pairs={{0,30},{2,0},{4,2},{6,4},{8,6},{10,8},{12,10},{14,12},{16,14},{18,... | collective-permute-start | bytes 49160 | tf_op jit(solution)/shard_map/ppermute | solution.py:25
  180.0 1.0 collective-permute-done.5
  181.0 4.4 %collective-permute-start.7 = (f32[1,4,1024]{2,1,0:T(4,128)S(1)}, f32[1,4,1024]{2,1,0:T(4,128)S(1)}, u32[]{:S(2)}, u32[]{:S(2)}) collective-permute-start(f32[1,4,1024]{2,1,0:T(4,128)S(1)} %collective-permute-done.5), channel_id=1, source_target_pairs={{0,30},{2,0},{4,2},{6,4},{8,6},{10,8},{12,10},{14,12},{16,14},{18,... | collective-permute-start | bytes 49160 | tf_op jit(solution)/shard_map/ppermute | solution.py:25
  185.8 1.0 collective-permute-done.7
  186.9 4.4 %collective-permute-start.9 = (f32[1,4,1024]{2,1,0:T(4,128)S(1)}, f32[1,4,1024]{2,1,0:T(4,128)S(1)}, u32[]{:S(2)}, u32[]{:S(2)}) collective-permute-start(f32[1,4,1024]{2,1,0:T(4,128)S(1)} %collective-permute-done.7), channel_id=1, source_target_pairs={{0,30},{2,0},{4,2},{6,4},{8,6},{10,8},{12,10},{14,12},{16,14},{18,... | collective-permute-start | bytes 49160 | tf_op jit(solution)/shard_map/ppermute | solution.py:25
  191.7 1.0 collective-permute-done.9
  192.7 4.4 %collective-permute-start.11 = (f32[1,4,1024]{2,1,0:T(4,128)S(1)}, f32[1,4,1024]{2,1,0:T(4,128)S(1)}, u32[]{:S(2)}, u32[]{:S(2)}) collective-permute-start(f32[1,4,1024]{2,1,0:T(4,128)S(1)} %collective-permute-done.9), channel_id=1, source_target_pairs={{0,30},{2,0},{4,2},{6,4},{8,6},{10,8},{12,10},{14,12},{16,14},{18,... | collective-permute-start | bytes 49160 | tf_op jit(solution)/shard_map/ppermute | solution.py:25
  197.2 0.3 collective-permute-done.10
  197.4 0.3 fusion.77
  197.7 0.9 collective-permute-done.11
  198.6 4.4 %collective-permute-start.13 = (f32[1,4,1024]{2,1,0:T(4,128)S(1)}, f32[1,4,1024]{2,1,0:T(4,128)S(1)}, u32[]{:S(2)}, u32[]{:S(2)}) collective-permute-start(f32[1,4,1024]{2,1,0:T(4,128)S(1)} %collective-permute-done.11), channel_id=1, source_target_pairs={{0,30},{2,0},{4,2},{6,4},{8,6},{10,8},{12,10},{14,12},{16,14},{18,... | collective-permute-start | bytes 49160 | tf_op jit(solution)/shard_map/ppermute | solution.py:25
  203.0 0.3 collective-permute-done.12
  203.5 1.2 fusion.29
  204.7 4.5 %collective-permute-start.15 = (f32[1,4,1024]{2,1,0:T(4,128)S(1)}, f32[1,4,1024]{2,1,0:T(4,128)S(1)}, u32[]{:S(2)}, u32[]{:S(2)}) collective-permute-start(f32[1,4,1024]{2,1,0:T(4,128)S(1)} %collective-permute-done.13), channel_id=1, source_target_pairs={{0,30},{2,0},{4,2},{6,4},{8,6},{10,8},{12,10},{14,12},{16,14},{18,... | collective-permute-start | bytes 49160 | tf_op jit(solution)/shard_map/ppermute | solution.py:25
  212.0 3.2 %collective-permute-done.16 = f32[1,4,1024]{2,1,0:T(4,128)S(1)} collective-permute-done((f32[1,4,1024]{2,1,0:T(4,128)S(1)}, f32[1,4,1024]{2,1,0:T(4,128)S(1)}, u32[]{:S(2)}, u32[]{:S(2)}) %collective-permute-start.16) | collective-permute-done | bytes 16416 | tf_op jit(solution)/shard_map/ppermute | solution.py:20
  218.3 13.7 %fusion.28 = f32[512,2048]{1,0:T(8,128)} fusion(bf16[1024,2048]{1,0:T(8,128)(2,1)} %param.26, f32[512,1024]{1,0:T(8,128)} %copy-done.4, f32[512,1024]{1,0:T(8,128)} %bitcast.135, f32[512,1024]{1,0:T(8,128)} %bitcast.139, f32[512,1024]{1,0:T(8,128)} %bitcast.137, bf16[2048,1024]{1,0:T(8,128)(2,1)} %param.17, f32[1024]{0:T(1024)S(1)} %bitcast.147, ...), kind=kOutput, calls=%fused_computation.63 | convolution fusion | flops 4308074496 | bytes 23087104 | tf_op jit(solution)/shard_map/dot_general | solution.py:50
  232.0 4.8 %add_convert_fusion = bf16[512,2048]{1,0:T(8,128)(2,1)} fusion(f32[512,2048]{1,0:T(8,128)} %fusion.28, bf16[512,512]{0,1:T(8,128)(2,1)S(1)} %fusion.27, bf16[512,2048]{1,0:T(8,128)(2,1)S(1)} %copy-done), kind=kOutput, calls=%fused_computation.12 | convolution fusion | flops 1075838976 | bytes 8912896 | tf_op jit(solution)/shard_map/dot_general | solution.py:50
  236.9 29.2 %reduce-scatter.2.cloned.1.call-done = bf16[256,2048]{1,0:T(8,128)(2,1)} async-done(((bf16[512,2048]{1,0:T(8,128)(2,1)}), bf16[256,2048]{1,0:T(8,128)(2,1)}) %reduce-scatter.2.cloned.1.call-update) | async-done | bytes 1048592 | tf_op jit(solution)/shard_map/reduce_scatter | solution.py:204
  (353 shorter events, 11.3 us)
Async XLA Ops:
  6.5 225.5 %copy-start = (bf16[512,2048]{1,0:T(8,128)(2,1)S(1)}, bf16[512,2048]{1,0:T(8,128)(2,1)}, u32[]{:S(2)}) copy-start(bf16[512,2048]{1,0:T(8,128)(2,1)} %param.27) | copy-start | bytes 6291460
  6.5 3.3 %copy-start.14 = (f32[2,512]{1,0:T(2,128)S(1)}, f32[2,512]{1,0:T(2,128)}, u32[]{:S(2)}) copy-start(f32[2,512]{1,0:T(2,128)} %param.22) | copy-start | bytes 12292
  6.5 3.3 %copy-start.13 = (f32[2,1024]{1,0:T(2,128)S(1)}, f32[2,1024]{1,0:T(2,128)}, u32[]{:S(2)}) copy-start(f32[2,1024]{1,0:T(2,128)} %param.21) | copy-start | bytes 24580
  6.5 3.4 %copy-start.12 = (bf16[4,1024]{1,0:T(4,128)(2,1)S(1)}, bf16[4,1024]{1,0:T(4,128)(2,1)}, u32[]{:S(2)}) copy-start(bf16[4,1024]{1,0:T(4,128)(2,1)} %param.19) | copy-start | bytes 24580
  6.5 38.2 %all-gather.2.cloned.1.call-start = ((), (), s32[]{:S(2)}) async-start(), calls=%async_computation.1 | async-start | bytes 3145728 | tf_op jit(solution)/shard_map/all_gather | solution.py:106
  7.3 258.8 %reduce-scatter.2.cloned.1.call-start = ((), (), s32[]{:S(2)}) async-start(), calls=%async_computation.2 | async-start | bytes 3145728 | tf_op jit(solution)/shard_map/reduce_scatter | solution.py:204
  44.7 2.2 copy-start.8
  47.0 7.7 %copy-start.17 = (bf16[2048,512]{1,0:T(8,128)(2,1)S(1)}, bf16[2048,512]{1,0:T(8,128)(2,1)}, u32[]{:S(2)}) copy-start(bf16[2048,512]{1,0:T(8,128)(2,1)} %param.18) | copy-start | bytes 6291460
  51.7 5.0 %collective-permute-start = (bf16[2,1024]{1,0:T(2,128)(2,1)S(1)}, bf16[2,1024]{1,0:T(2,128)(2,1)S(1)}, u32[]{:S(2)}, u32[]{:S(2)}) collective-permute-start(bf16[2,1024]{1,0:T(2,128)(2,1)S(1)} %get-tuple-element.22), channel_id=1, source_target_pairs={{0,2},{2,4},{4,6},{6,8},{8,10},{10,12},{12,14},{14,16},{16,18},{18... | collective-permute-start | bytes 12296 | tf_op jit(solution)/shard_map/ppermute | solution.py:37
  53.3 4.5 %collective-permute-start.1 = (bf16[2,1024]{1,0:T(2,128)(2,1)S(1)}, bf16[2,1024]{1,0:T(2,128)(2,1)S(1)}, u32[]{:S(2)}, u32[]{:S(2)}) collective-permute-start(bf16[2,1024]{1,0:T(2,128)(2,1)S(1)} %get-tuple-element.23), channel_id=1, source_target_pairs={{2,0},{4,2},{6,4},{8,6},{10,8},{12,10},{14,12},{16,14},{18,16},{20... | collective-permute-start | bytes 12296 | tf_op jit(solution)/shard_map/ppermute | solution.py:40
  77.0 5.4 %copy-start.15 = (f32[2,512]{1,0:T(2,128)S(1)}, f32[2,512]{1,0:T(2,128)}, u32[]{:S(2)}) copy-start(f32[2,512]{1,0:T(2,128)} %param.23) | copy-start | bytes 12292
  89.6 3.9 %copy-start.1 = (f32[512,2,1024]{2,0,1:T(8,128)}, f32[512,2,1024]{2,0,1:T(8,128)S(1)}, u32[]{:S(2)}) copy-start(f32[512,2,1024]{2,0,1:T(8,128)S(1)} %get-tuple-element.6) | copy-start | bytes 12582916
  98.6 3.0 %copy-start.10 = (f32[512,1,1024]{2,0,1:T(8,128)S(1)}, f32[512,1,1024]{2,0,1:T(8,128)}, u32[]{:S(2)}) copy-start(f32[512,1,1024]{2,0,1:T(8,128)} %get-tuple-element.98) | copy-start | bytes 6291460
  113.9 1.3 copy-start.2
  121.1 3.0 %copy-start.9 = (f32[512,1,1024]{2,0,1:T(8,128)S(1)}, f32[512,1,1024]{2,0,1:T(8,128)}, u32[]{:S(2)}) copy-start(f32[512,1,1024]{2,0,1:T(8,128)} %get-tuple-element.99) | copy-start | bytes 6291460
  136.2 1.3 copy-start.3
  149.1 1.4 copy-start.5
  153.6 1.4 copy-start.4
  160.8 1.3 copy-start.6
  160.8 5.1 %copy-start.11 = (bf16[512,512]{1,0:T(8,128)(2,1)S(1)}, bf16[512,512]{1,0:T(8,128)(2,1)}, u32[]{:S(2)}) copy-start(bf16[512,512]{1,0:T(8,128)(2,1)} %convolution_convert_fusion.2) | copy-start | bytes 1572868
  160.8 9.3 %copy-start.16 = (bf16[512]{0:T(512)(128)(2,1)S(1)}, bf16[512]{0:T(512)(128)(2,1)}, u32[]{:S(2)}) copy-start(bf16[512]{0:T(512)(128)(2,1)} %param.25) | copy-start | bytes 3076
  162.1 1.4 copy-start.7
  163.5 10.4 %collective-permute-start.2 = (f32[1,4,1024]{2,1,0:T(4,128)S(1)}, f32[1,4,1024]{2,1,0:T(4,128)S(1)}, u32[]{:S(2)}, u32[]{:S(2)}) collective-permute-start(f32[1,4,1024]{2,1,0:T(4,128)S(1)} %maximum_bitcast_fusion), channel_id=1, source_target_pairs={{0,2},{2,4},{4,6},{6,8},{8,10},{10,12},{12,14},{14,16},{16,18},{18... | collective-permute-start | bytes 49160 | tf_op jit(solution)/shard_map/ppermute | solution.py:20
  165.9 8.1 %collective-permute-start.17 = (bf16[8,512]{1,0:T(8,128)(2,1)S(1)}, bf16[8,512]{1,0:T(8,128)(2,1)S(1)}, u32[]{:S(2)}, u32[]{:S(2)}) collective-permute-start(bf16[8,512]{1,0:T(8,128)(2,1)S(1)} %get-tuple-element.24), channel_id=1, source_target_pairs={{0,2},{2,4},{4,6},{6,8},{8,10},{10,12},{12,14},{14,16},{16,18},{18... | collective-permute-start | bytes 24584 | tf_op jit(solution)/shard_map/ppermute | solution.py:37
  168.6 5.3 %collective-permute-start.18 = (bf16[8,512]{1,0:T(8,128)(2,1)S(1)}, bf16[8,512]{1,0:T(8,128)(2,1)S(1)}, u32[]{:S(2)}, u32[]{:S(2)}) collective-permute-start(bf16[8,512]{1,0:T(8,128)(2,1)S(1)} %get-tuple-element.25), channel_id=1, source_target_pairs={{2,0},{4,2},{6,4},{8,6},{10,8},{12,10},{14,12},{16,14},{18,16},{20... | collective-permute-start | bytes 24584 | tf_op jit(solution)/shard_map/ppermute | solution.py:40
  170.2 4.9 %collective-permute-start.3 = (f32[1,4,1024]{2,1,0:T(4,128)S(1)}, f32[1,4,1024]{2,1,0:T(4,128)S(1)}, u32[]{:S(2)}, u32[]{:S(2)}) collective-permute-start(f32[1,4,1024]{2,1,0:T(4,128)S(1)} %maximum_bitcast_fusion), channel_id=1, source_target_pairs={{0,30},{2,0},{4,2},{6,4},{8,6},{10,8},{12,10},{14,12},{16,14},{18,... | collective-permute-start | bytes 49160 | tf_op jit(solution)/shard_map/ppermute | solution.py:25
  173.9 5.9 %collective-permute-start.4 = (f32[1,4,1024]{2,1,0:T(4,128)S(1)}, f32[1,4,1024]{2,1,0:T(4,128)S(1)}, u32[]{:S(2)}, u32[]{:S(2)}) collective-permute-start(f32[1,4,1024]{2,1,0:T(4,128)S(1)} %collective-permute-done.2), channel_id=1, source_target_pairs={{0,2},{2,4},{4,6},{6,8},{8,10},{10,12},{12,14},{14,16},{16,18},{18... | collective-permute-start | bytes 49160 | tf_op jit(solution)/shard_map/ppermute | solution.py:20
  175.1 5.9 %collective-permute-start.5 = (f32[1,4,1024]{2,1,0:T(4,128)S(1)}, f32[1,4,1024]{2,1,0:T(4,128)S(1)}, u32[]{:S(2)}, u32[]{:S(2)}) collective-permute-start(f32[1,4,1024]{2,1,0:T(4,128)S(1)} %collective-permute-done.3), channel_id=1, source_target_pairs={{0,30},{2,0},{4,2},{6,4},{8,6},{10,8},{12,10},{14,12},{16,14},{18,... | collective-permute-start | bytes 49160 | tf_op jit(solution)/shard_map/ppermute | solution.py:25
  179.8 5.9 %collective-permute-start.6 = (f32[1,4,1024]{2,1,0:T(4,128)S(1)}, f32[1,4,1024]{2,1,0:T(4,128)S(1)}, u32[]{:S(2)}, u32[]{:S(2)}) collective-permute-start(f32[1,4,1024]{2,1,0:T(4,128)S(1)} %collective-permute-done.4), channel_id=1, source_target_pairs={{0,2},{2,4},{4,6},{6,8},{8,10},{10,12},{12,14},{14,16},{16,18},{18... | collective-permute-start | bytes 49160 | tf_op jit(solution)/shard_map/ppermute | solution.py:20
  181.0 5.9 %collective-permute-start.7 = (f32[1,4,1024]{2,1,0:T(4,128)S(1)}, f32[1,4,1024]{2,1,0:T(4,128)S(1)}, u32[]{:S(2)}, u32[]{:S(2)}) collective-permute-start(f32[1,4,1024]{2,1,0:T(4,128)S(1)} %collective-permute-done.5), channel_id=1, source_target_pairs={{0,30},{2,0},{4,2},{6,4},{8,6},{10,8},{12,10},{14,12},{16,14},{18,... | collective-permute-start | bytes 49160 | tf_op jit(solution)/shard_map/ppermute | solution.py:25
  185.7 5.9 %collective-permute-start.8 = (f32[1,4,1024]{2,1,0:T(4,128)S(1)}, f32[1,4,1024]{2,1,0:T(4,128)S(1)}, u32[]{:S(2)}, u32[]{:S(2)}) collective-permute-start(f32[1,4,1024]{2,1,0:T(4,128)S(1)} %collective-permute-done.6), channel_id=1, source_target_pairs={{0,2},{2,4},{4,6},{6,8},{8,10},{10,12},{12,14},{14,16},{16,18},{18... | collective-permute-start | bytes 49160 | tf_op jit(solution)/shard_map/ppermute | solution.py:20
  186.9 5.9 %collective-permute-start.9 = (f32[1,4,1024]{2,1,0:T(4,128)S(1)}, f32[1,4,1024]{2,1,0:T(4,128)S(1)}, u32[]{:S(2)}, u32[]{:S(2)}) collective-permute-start(f32[1,4,1024]{2,1,0:T(4,128)S(1)} %collective-permute-done.7), channel_id=1, source_target_pairs={{0,30},{2,0},{4,2},{6,4},{8,6},{10,8},{12,10},{14,12},{16,14},{18,... | collective-permute-start | bytes 49160 | tf_op jit(solution)/shard_map/ppermute | solution.py:25
  191.6 5.9 %collective-permute-start.10 = (f32[1,4,1024]{2,1,0:T(4,128)S(1)}, f32[1,4,1024]{2,1,0:T(4,128)S(1)}, u32[]{:S(2)}, u32[]{:S(2)}) collective-permute-start(f32[1,4,1024]{2,1,0:T(4,128)S(1)} %collective-permute-done.8), channel_id=1, source_target_pairs={{0,2},{2,4},{4,6},{6,8},{8,10},{10,12},{12,14},{14,16},{16,18},{18... | collective-permute-start | bytes 49160 | tf_op jit(solution)/shard_map/ppermute | solution.py:20
  191.7 11.8 %copy-start.18 = (bf16[4,128,128]{2,1,0:T(8,128)(2,1)S(1)}, bf16[4,128,128]{2,1,0:T(8,128)(2,1)}, u32[]{:S(2)}) copy-start(bf16[4,128,128]{2,1,0:T(8,128)(2,1)} %param.24) | copy-start | bytes 393220
  192.7 5.9 %collective-permute-start.11 = (f32[1,4,1024]{2,1,0:T(4,128)S(1)}, f32[1,4,1024]{2,1,0:T(4,128)S(1)}, u32[]{:S(2)}, u32[]{:S(2)}) collective-permute-start(f32[1,4,1024]{2,1,0:T(4,128)S(1)} %collective-permute-done.9), channel_id=1, source_target_pairs={{0,30},{2,0},{4,2},{6,4},{8,6},{10,8},{12,10},{14,12},{16,14},{18,... | collective-permute-start | bytes 49160 | tf_op jit(solution)/shard_map/ppermute | solution.py:25
  197.4 5.9 %collective-permute-start.12 = (f32[1,4,1024]{2,1,0:T(4,128)S(1)}, f32[1,4,1024]{2,1,0:T(4,128)S(1)}, u32[]{:S(2)}, u32[]{:S(2)}) collective-permute-start(f32[1,4,1024]{2,1,0:T(4,128)S(1)} %collective-permute-done.10), channel_id=1, source_target_pairs={{0,2},{2,4},{4,6},{6,8},{8,10},{10,12},{12,14},{14,16},{16,18},{18... | collective-permute-start | bytes 49160 | tf_op jit(solution)/shard_map/ppermute | solution.py:20
  198.6 6.1 %collective-permute-start.13 = (f32[1,4,1024]{2,1,0:T(4,128)S(1)}, f32[1,4,1024]{2,1,0:T(4,128)S(1)}, u32[]{:S(2)}, u32[]{:S(2)}) collective-permute-start(f32[1,4,1024]{2,1,0:T(4,128)S(1)} %collective-permute-done.11), channel_id=1, source_target_pairs={{0,30},{2,0},{4,2},{6,4},{8,6},{10,8},{12,10},{14,12},{16,14},{18,... | collective-permute-start | bytes 49160 | tf_op jit(solution)/shard_map/ppermute | solution.py:25
  203.3 6.0 %collective-permute-start.14 = (f32[1,4,1024]{2,1,0:T(4,128)S(1)}, f32[1,4,1024]{2,1,0:T(4,128)S(1)}, u32[]{:S(2)}, u32[]{:S(2)}) collective-permute-start(f32[1,4,1024]{2,1,0:T(4,128)S(1)} %collective-permute-done.12), channel_id=1, source_target_pairs={{0,2},{2,4},{4,6},{6,8},{8,10},{10,12},{12,14},{14,16},{16,18},{18... | collective-permute-start | bytes 49160 | tf_op jit(solution)/shard_map/ppermute | solution.py:20
  204.7 7.1 %collective-permute-start.15 = (f32[1,4,1024]{2,1,0:T(4,128)S(1)}, f32[1,4,1024]{2,1,0:T(4,128)S(1)}, u32[]{:S(2)}, u32[]{:S(2)}) collective-permute-start(f32[1,4,1024]{2,1,0:T(4,128)S(1)} %collective-permute-done.13), channel_id=1, source_target_pairs={{0,30},{2,0},{4,2},{6,4},{8,6},{10,8},{12,10},{14,12},{16,14},{18,... | collective-permute-start | bytes 49160 | tf_op jit(solution)/shard_map/ppermute | solution.py:25
  209.3 5.9 %collective-permute-start.16 = (f32[1,4,1024]{2,1,0:T(4,128)S(1)}, f32[1,4,1024]{2,1,0:T(4,128)S(1)}, u32[]{:S(2)}, u32[]{:S(2)}) collective-permute-start(f32[1,4,1024]{2,1,0:T(4,128)S(1)} %collective-permute-done.14), channel_id=1, source_target_pairs={{0,2},{2,4},{4,6},{6,8},{8,10},{10,12},{12,14},{14,16},{16,18},{18... | collective-permute-start | bytes 49160 | tf_op jit(solution)/shard_map/ppermute | solution.py:20
Sparse Core Ops, SparseCore 0:
  8.9 35.8 all-gather.1
  237.0 28.9 reduce-scatter.1
